TPU v7x, 32 devices: a whole 2x2x4 slice. The times are simulated.
32 devices in a mesh: sp: 8 (over z, x), tp: 4 (over y, core).
Axes of the slice: x: 2, y: 2, z: 4, core: 2. Of those that a mesh axis runs over, the one named last changes fastest.
Arguments:
- residual: bfloat16 [6144, 2048], P('sp'), may hold values from -6 to 6
- query_matrix: bfloat16 [6144, 1024], P('sp', 'tp'), may hold values from -6 to 6
- key_matrix: bfloat16 [6144, 1024], P('sp', 'tp'), may hold values from -6 to 6
- value_matrix: bfloat16 [6144, 2048], P('sp', 'tp'), may hold values from -6 to 6
- output_gate_logit: bfloat16 [6144, 2048], P('sp', 'tp'), may hold values from -6 to 6
- input_gate_log: float32 [6144, 8], P('sp', 'tp'), may hold values from -4 to 125
- forget_gate_logit: float32 [6144, 8], P('sp', 'tp')
- extra_head_decay: float32 [6144, 8], P('sp', 'tp'), may hold values from -1 to 0
- head_norm_gain: float32 [2048], P('tp'), may hold values from 0.1 to 1.9
- projection: bfloat16 [2048, 2048], P('tp'), may hold values from -5.303301 to 5.303301
- cell_output_gain: float32 [2048], replicated, may hold values from 0.1 to 1.9
- mixer_input_gain: float32 [2048], replicated, may hold values from 0.1 to 1.9
- mixer_gate_weight: bfloat16 [2048, 5120], P('sp', 'tp'), may hold values from -0.125 to 0.125
- mixer_up_weight: bfloat16 [2048, 5120], P('sp', 'tp'), may hold values from -0.125 to 0.125
- mixer_down_weight: bfloat16 [5120, 2048], P('tp', 'sp'), may hold values from -0.078125 to 0.078125
Outputs:
- updated: bfloat16 [6144, 2048], P('sp', 'tp')
All inputs are finite; a program needn't handle non-finite values.
Results may differ from a plain program's by a relative error of at most 0.014.
Values may be sent and summed in bfloat16 or wider, within the bound.
A program may use at most 128 MiB of HBM per device.

v0:
```python
import jax
import jax.numpy as jnp
from jax import lax
from jax.sharding import PartitionSpec as P

DQK = 128
DV = 256
HIGHEST = lax.Precision.HIGHEST
EPSILON = 1e-06
LOWEST_LOG = -1e30


def carried_in(value, axis, join, neutral):
    count, mine = (lax.axis_size(axis), lax.axis_index(axis))
    pieces = jax.tree.map(lambda part: lax.all_gather(part, axis), value)
    subtotal = jax.tree.map(
        lambda part, zero: jnp.full_like(part, 0) + jnp.asarray(zero, part.dtype), value, neutral
    )

    def turn(position, subtotal):
        longer = join(subtotal, jax.tree.map(lambda part: part[position], pieces))
        return jax.tree.map(lambda new, old: jnp.where(position < mine, new, old), longer, subtotal)

    return lax.fori_loop(0, count - 1, turn, subtotal)


def heads_first(array, heads, width):
    return array.reshape(array.shape[0], heads, width).transpose(1, 0, 2)


def read_out(
    query_low, key_low, value_low, in_logs, running_log_total, memory, normalizer, stabilizer
):
    length = query_low.shape[1]
    causal = lax.broadcasted_iota(jnp.int32, (length, length), 0) >= lax.broadcasted_iota(
        jnp.int32, (length, length), 1
    )
    spread = running_log_total[:, :, None] - running_log_total[:, None, :] + in_logs[:, None, :]
    spread = jnp.where(causal[None], spread, -jnp.inf)
    carried = running_log_total + stabilizer[:, None]
    running = jnp.maximum(carried, jnp.max(spread, axis=-1))
    scores = jnp.einsum(
        "htd,hsd->hts", query_low, key_low, preferred_element_type=jnp.float32
    ) * DQK ** (-0.5)
    weights = jnp.exp(spread - running[:, :, None]) * scores
    scaled = jnp.exp(carried - running)
    scaled_query = query_low.astype(jnp.float32) * DQK ** (-0.5)
    numerator = jnp.einsum(
        "hts,hsv->htv", weights.astype(jnp.bfloat16), value_low, preferred_element_type=jnp.float32
    )
    numerator = numerator + scaled[:, :, None] * jnp.einsum(
        "hvd,htd->htv", memory, scaled_query, precision=HIGHEST
    )
    denominator = jnp.sum(weights, axis=-1) + scaled * jnp.einsum(
        "hd,htd->ht", normalizer, scaled_query, precision=HIGHEST
    )
    return numerator / jnp.maximum(jnp.abs(denominator), jnp.exp(-running))[:, :, None]


def fold_state(keyed, valued, in_logs, running_log_total, memory, normalizer, stabilizer):
    last = running_log_total[:, -1]
    lifted = last[:, None] - running_log_total + in_logs
    new_max = jnp.maximum(last + stabilizer, jnp.max(lifted, axis=-1))
    weights = jnp.exp(lifted - new_max[:, None])
    retained = jnp.exp(last + stabilizer - new_max)
    memory = retained[:, None, None] * memory + jnp.einsum(
        "hsv,hsd->hvd", weights[:, :, None] * valued, keyed, precision=HIGHEST
    )
    normalizer = retained[:, None] * normalizer + jnp.einsum(
        "hs,hsd->hd", weights, keyed, precision=HIGHEST
    )
    return (memory, normalizer, new_max)


def join_states(earlier, later):
    early_decay, early_memory, early_normalizer, early_max = earlier
    late_decay, late_memory, late_normalizer, late_max = later
    joined_max = jnp.maximum(late_decay + early_max, late_max)
    first_scale = jnp.exp(late_decay + early_max - joined_max)
    second_scale = jnp.exp(late_max - joined_max)
    memory = first_scale[:, None, None] * early_memory + second_scale[:, None, None] * late_memory
    normalizer = first_scale[:, None] * early_normalizer + second_scale[:, None] * late_normalizer
    return (early_decay + late_decay, memory, normalizer, joined_max)


def body(
    residual,
    query_matrix,
    key_matrix,
    value_matrix,
    output_gate_logit,
    input_gate_log,
    forget_gate_logit,
    extra_head_decay,
    head_norm_gain,
    projection,
    cell_output_gain,
    mixer_input_gain,
    mixer_gate_weight,
    mixer_up_weight,
    mixer_down_weight,
):
    tok_rows = residual.shape[0]
    width = residual.shape[1]
    heads_here = input_gate_log.shape[1]
    query_low = heads_first(query_matrix, heads_here, DQK)
    key_low = heads_first(key_matrix, heads_here, DQK)
    value_low = heads_first(value_matrix, heads_here, DV)
    keyed = key_low.astype(jnp.float32)
    valued = value_low.astype(jnp.float32)
    in_logs = input_gate_log.T
    running_log_total = jnp.cumsum(
        (jax.nn.log_sigmoid(forget_gate_logit) + extra_head_decay).T, axis=-1
    )
    zero_memory = jnp.zeros((heads_here, DV, DQK), jnp.float32)
    zero_normalizer = jnp.zeros((heads_here, DQK), jnp.float32)
    lowest = jnp.full((heads_here,), LOWEST_LOG, jnp.float32)
    local_memory, local_normalizer, local_max = fold_state(
        keyed, valued, in_logs, running_log_total, zero_memory, zero_normalizer, lowest
    )
    prior_decay, prior_memory, prior_normalizer, prior_max = carried_in(
        (running_log_total[:, -1], local_memory, local_normalizer, local_max),
        "sp",
        join_states,
        (jnp.zeros_like(lowest), zero_memory, zero_normalizer, lowest),
    )
    start_max = jnp.maximum(prior_decay, prior_max)
    lift = jnp.exp(prior_max - start_max)
    cells = read_out(
        query_low,
        key_low,
        value_low,
        in_logs,
        running_log_total,
        lift[:, None, None] * prior_memory,
        lift[:, None] * prior_normalizer,
        start_max,
    )
    centered = cells - jnp.mean(cells, axis=-1, keepdims=True)
    normed = centered * lax.rsqrt(jnp.mean(centered * centered, axis=-1, keepdims=True) + EPSILON)
    normed = normed * head_norm_gain.reshape(heads_here, DV)[:, None, :]
    normed = normed.transpose(1, 0, 2).reshape(tok_rows, heads_here * DV)
    gated = (normed * jax.nn.sigmoid(output_gate_logit.astype(jnp.float32))).astype(jnp.bfloat16)
    cols_here = width // lax.axis_size("tp")
    offset = lax.axis_index("tp") * cols_here
    columns = projection
    mixed = (
        lax.psum_scatter(
            lax.dot_general(
                columns, gated, (((0,), (1,)), ((), ())), preferred_element_type=jnp.float32
            ).astype(jnp.bfloat16),
            "tp",
            scatter_dimension=0,
            tiled=True,
        )
        .astype(jnp.float32)
        .T
    )
    squares = lax.psum(jnp.sum(mixed * mixed, axis=-1), "tp")
    mixed = (
        mixed
        * lax.rsqrt(squares / width + EPSILON)[:, None]
        * lax.dynamic_slice_in_dim(cell_output_gain, offset, cols_here, 0)
    )
    own_residual = lax.dynamic_slice_in_dim(residual, offset, cols_here, 1).astype(jnp.float32)
    first_sum = (own_residual + mixed).astype(jnp.bfloat16)
    own_first = lax.optimization_barrier(first_sum).astype(jnp.float32)
    first_total = lax.psum(jnp.sum(own_first * own_first, axis=-1), "tp")
    own_gain = lax.dynamic_slice_in_dim(mixer_input_gain, offset, cols_here, 0)
    normed_own = (own_first * lax.rsqrt(first_total / width + EPSILON)[:, None] * own_gain).astype(
        jnp.bfloat16
    )
    normed_rows = lax.all_gather(normed_own, "tp", axis=1, tiled=True)
    columns = normed_rows
    gate_value = jnp.dot(
        columns,
        lax.all_gather(mixer_gate_weight, "sp", axis=0, tiled=True),
        preferred_element_type=jnp.float32,
    )
    up_value = jnp.dot(
        columns,
        lax.all_gather(mixer_up_weight, "sp", axis=0, tiled=True),
        preferred_element_type=jnp.float32,
    )
    activated = (jax.nn.silu(gate_value) * up_value).astype(jnp.bfloat16)
    down_terms = jnp.dot(
        activated,
        lax.all_gather(mixer_down_weight, "sp", axis=1, tiled=True),
        preferred_element_type=jnp.float32,
    )
    channel_out = lax.psum_scatter(
        down_terms.astype(jnp.bfloat16), "tp", scatter_dimension=1, tiled=True
    ).astype(jnp.float32)
    return (own_first + 0.5 * channel_out).astype(jnp.bfloat16)


def solution(mesh):
    return jax.shard_map(
        body,
        mesh=mesh,
        in_specs=(
            P("sp", None),
            P("sp", "tp"),
            P("sp", "tp"),
            P("sp", "tp"),
            P("sp", "tp"),
            P("sp", "tp"),
            P("sp", "tp"),
            P("sp", "tp"),
            P("tp"),
            P("tp", None),
            P(),
            P(),
            P("sp", "tp"),
            P("sp", "tp"),
            P("tp", "sp"),
        ),
        out_specs=P("sp", "tp"),
        check_vma=False,
    )
```

profile of v0, /device:TPU:0, one launch (start us, length us, event | category | flops | bytes accessed | tf_op | source)
XLA Modules:
  0.0 489.8 jit_solution(3324282672585852311)
XLA Ops:
  9.9 1.4 copy.54
  11.4 2.8 fusion.32
  15.8 22.4 %all-gather.3 = f32[8,1,2]{2,1,0:T(1,128)S(1)} all-gather(f32[1,1,2]{2,1,0:T(1,128)S(1)} %fusion.59), channel_id=1, replica_groups=mesh['sp'=8,'tp'=4] {'sp'}, dimensions={0}, use_global_device_ids=true | all-gather | bytes 72 | tf_op jit(solution)/shard_map/all_gather | solution.py:15
  38.1 17.6 %all-reduce = f32[16]{0:T(128)S(1)} all-reduce(f32[16]{0:T(128)S(1)} %dynamic-update-slice), channel_id=2, replica_groups=mesh['sp'=8,'tp'=4] {'sp'}, use_global_device_ids=true, to_apply=%add | all-reduce | flops 16 | bytes 128
  56.2 18.9 %all-gather.4 = f32[8,2,128]{2,1,0:T(2,128)S(1)} all-gather(f32[1,2,128]{2,1,0:T(2,128)S(1)} %add_bitcast_fusion.1), channel_id=4, replica_groups=mesh['sp'=8,'tp'=4] {'sp'}, dimensions={0}, use_global_device_ids=true | all-gather | bytes 9216 | tf_op jit(solution)/shard_map/all_gather | solution.py:15
  76.4 8.3 %while.20 = (s32[]{:T(128)}, f32[2]{0:T(128)S(1)}, f32[2,256,128]{2,1,0:T(8,128)S(1)}, f32[2,128]{1,0:T(2,128)S(1)}, f32[2]{0:T(128)S(1)}, /*index=5*/s32[]{:T(1...) while((s32[]{:T(128)}, f32[2]{0:T(128)S(1)}, ...), condition=%wide.region_4.5_spmd.clone, body=%wide.region_3.4_spmd.clone.sunk | while | flops 328984 | bytes 789781 | solution.py:24
  76.4 1.1 fusion.90
  77.6 1.1 fusion.90
  78.8 1.1 fusion.90
  80.0 1.1 fusion.90
  81.2 1.1 fusion.90
  82.4 1.1 fusion.90
  84.8 3.0 fusion.10
  88.5 1.5 fusion.37
  90.1 2.4 fusion.69
  92.9 1.5 fusion.28
  94.4 3.1 copy.47
  97.5 4.9 fusion.9
  104.7 32.8 %reduce-scatter.3.cloned.1.call-done = bf16[512,768]{0,1:T(8,128)(2,1)} async-done(((bf16[2048,768]{0,1:T(8,128)(2,1)}), bf16[512,768]{0,1:T(8,128)(2,1)}) %reduce-scatter.3.cloned.1.call-update) | async-done | bytes 786448 | tf_op jit(solution)/shard_map/reduce_scatter | solution.py:148
  137.6 1.4 fusion.15
  138.9 5.8 %psum.14 = f32[768]{0:T(1024)S(1)} all-reduce(f32[768]{0:T(1024)S(1)} %fusion.15), channel_id=1, replica_groups=mesh['sp'=8,'tp'=4] {'tp'}, use_global_device_ids=true, to_apply=%region_11.12 | all-reduce | flops 768 | bytes 6144 | tf_op jit(solution)/shard_map/psum | solution.py:159
  144.7 1.7 fusion.19
  146.7 5.7 %psum.15 = f32[768]{0:T(1024)S(1)} all-reduce(f32[768]{0:T(1024)S(1)} %fusion.20), channel_id=1, replica_groups=mesh['sp'=8,'tp'=4] {'tp'}, use_global_device_ids=true, to_apply=%region_13.14 | all-reduce | flops 768 | bytes 6144 | tf_op jit(solution)/shard_map/psum | solution.py:168
  152.3 1.1 fusion.22
  154.9 70.8 %all-gather.13.cloned.1.call-done = bf16[2048,1280]{1,0:T(8,128)(2,1)} async-done(((bf16[256,1280]{1,0:T(8,128)(2,1)}), bf16[2048,1280]{1,0:T(8,128)(2,1)}) %all-gather.13.cloned.1.call-update) | async-done | bytes 5242896 | tf_op jit(solution)/shard_map/all_gather | solution.py:177
  225.7 28.1 %all-gather.11.cloned.1.call-done = bf16[768,2048]{1,0:T(8,128)(2,1)} async-done(((bf16[768,512]{1,0:T(8,128)(2,1)}), bf16[768,2048]{1,0:T(8,128)(2,1)}) %all-gather.11.cloned.1.call-update) | async-done | bytes 3145744 | tf_op jit(solution)/shard_map/all_gather | solution.py:173
  253.8 9.6 %fusion.72 = f32[768,1280]{1,0:T(8,128)} fusion(bf16[768,2048]{1,0:T(8,128)(2,1)} %all-gather.11.cloned.1.call-done, bf16[2048,1280]{1,0:T(8,128)(2,1)} %all-gather.13.cloned.1.call-done), kind=kOutput, calls=%fused_computation.118 | convolution fusion | flops 4026531840 | bytes 12320768 | tf_op jit(solution)/shard_map/dot_general | solution.py:175
  263.4 78.4 %all-gather.15.cloned.1.call-done = bf16[2048,1280]{1,0:T(8,128)(2,1)} async-done(((bf16[256,1280]{1,0:T(8,128)(2,1)}), bf16[2048,1280]{1,0:T(8,128)(2,1)}) %all-gather.15.cloned.1.call-update) | async-done | bytes 5242896 | tf_op jit(solution)/shard_map/all_gather | solution.py:182
  341.8 86.9 %all-gather.17.cloned.1.call-done = bf16[1280,2048]{1,0:T(8,128)(2,1)} async-done(((bf16[1280,256]{1,0:T(8,128)(2,1)}), bf16[1280,2048]{1,0:T(8,128)(2,1)}) %all-gather.17.cloned.1.call-update) | async-done | bytes 5242896 | tf_op jit(solution)/shard_map/all_gather | solution.py:188
  428.7 16.0 %convolution_convert_fusion.1 = bf16[768,2048]{1,0:T(8,128)(2,1)} fusion(bf16[1280,2048]{1,0:T(8,128)(2,1)} %all-gather.17.cloned.1.call-done, bf16[768,2048]{1,0:T(8,128)(2,1)} %all-gather.11.cloned.1.call-done, bf16[2048,1280]{1,0:T(8,128)(2,1)} %all-gather.15.cloned.1.call-done, f32[768,1280]{1,0:T(8,128)} %fusion.72), kind=kOutput, calls=%fused_computation.23 | convolution fusion | flops 8060534784 | bytes 20709376 | tf_op jit(solution)/shard_map/dot_general | solution.py:186
  444.7 36.1 %reduce-scatter.5.cloned.1.call-done = bf16[768,512]{1,0:T(8,128)(2,1)} async-done(((bf16[768,2048]{1,0:T(8,128)(2,1)}), bf16[768,512]{1,0:T(8,128)(2,1)}) %reduce-scatter.5.cloned.1.call-update) | async-done | bytes 786448 | tf_op jit(solution)/shard_map/reduce_scatter | solution.py:191
  480.7 2.2 fusion.23
  (96 shorter events, 13.1 us)
Async XLA Ops:
  6.5 91.0 %copy-start = (bf16[512,2048]{1,0:T(8,128)(2,1)S(1)}, bf16[512,2048]{1,0:T(8,128)(2,1)}, u32[]{:S(2)}) copy-start(bf16[512,2048]{1,0:T(8,128)(2,1)} %param.26) | copy-start | bytes 6291460
  6.5 7.8 %copy-start.8 = (u32[32]{0:T(128)S(1)}, u32[32]{0:T(128)}, u32[]{:S(2)}) copy-start(u32[32]{0:T(128)} %constant.77) | copy-start | bytes 388
  6.5 49.4 %copy-start.4 = (bf16[768,256]{1,0:T(8,128)(2,1)S(1)}, bf16[768,256]{1,0:T(8,128)(2,1)}, u32[]{:S(2)}) copy-start(bf16[768,256]{1,0:T(8,128)(2,1)} %param.19) | copy-start | bytes 1179652
  6.5 49.3 %copy-start.6 = (f32[512]{0:T(512)S(1)}, f32[512]{0:T(512)}, u32[]{:S(2)}) copy-start(f32[512]{0:T(512)} %param.25) | copy-start | bytes 6148
  6.5 69.8 %all-gather.19.cloned.1.call-start = ((), (), s32[]{:S(2)}) async-start(), calls=%async_computation.8 | async-start | bytes 2359296 | tf_op jit(solution)/shard_map/all_gather | solution.py:15
  7.5 67.9 %copy-start.5 = (f32[768,2]{0,1:T(2,128)S(1)}, f32[768,2]{0,1:T(2,128)}, u32[]{:S(2)}) copy-start(f32[768,2]{0,1:T(2,128)} %param.22) | copy-start | bytes 18436
  11.3 26.8 %copy-start.1 = (bf16[768,512]{0,1:T(8,128)(2,1)}, bf16[768,512]{0,1:T(8,128)(2,1)S(1)}, u32[]{:S(2)}) copy-start(bf16[768,512]{0,1:T(8,128)(2,1)S(1)} %copy.54) | copy-start | bytes 2359300
  14.3 123.3 %reduce-scatter.3.cloned.1.call-start = ((), (), s32[]{:S(2)}) async-start(), calls=%async_computation.2 | async-start | bytes 3932160 | tf_op jit(solution)/shard_map/reduce_scatter | solution.py:148
  75.4 9.4 %copy-start.3 = (bf16[768,256]{1,0:T(8,128)(2,1)S(1)}, bf16[768,256]{1,0:T(8,128)(2,1)}, u32[]{:S(2)}) copy-start(bf16[768,256]{1,0:T(8,128)(2,1)} %param.18) | copy-start | bytes 1179652
  87.7 2.4 copy-start.2
  94.4 3.1 copy-start.7
  102.4 123.3 %all-gather.13.cloned.1.call-start = ((), (), s32[]{:S(2)}) async-start(), calls=%async_computation.4 | async-start | bytes 5898240 | tf_op jit(solution)/shard_map/all_gather | solution.py:177
  103.2 150.7 %all-gather.11.cloned.1.call-start = ((), (), s32[]{:S(2)}) async-start(), calls=%async_computation.3 | async-start | bytes 3932160 | tf_op jit(solution)/shard_map/all_gather | solution.py:173
  153.5 188.3 %all-gather.15.cloned.1.call-start = ((), (), s32[]{:S(2)}) async-start(), calls=%async_computation.5 | async-start | bytes 5898240 | tf_op jit(solution)/shard_map/all_gather | solution.py:182
  154.1 274.6 %all-gather.17.cloned.1.call-start = ((), (), s32[]{:S(2)}) async-start(), calls=%async_computation.6 | async-start | bytes 5898240 | tf_op jit(solution)/shard_map/all_gather | solution.py:188
  154.7 326.0 %reduce-scatter.5.cloned.1.call-start = ((), (), s32[]{:S(2)}) async-start(), calls=%async_computation.7 | async-start | bytes 3932160 | tf_op jit(solution)/shard_map/reduce_scatter | solution.py:191
Sparse Core Ops, SparseCore 0:
  14.4 52.0 all-gather.18
  102.5 34.9 reduce-scatter.2
  139.8 85.8 all-gather.12
  227.1 26.6 all-gather.10
  255.9 85.8 all-gather.14
  343.7 84.9 all-gather.16
  444.8 35.8 reduce-scatter.4
where the time goes:
time: 491 us; the launch traced here: 490 us
  waiting for transfers between devices  335 us (68%)
  blocking collectives  70.3 us (14%)
  matrix products  41 us (8%)
  other arithmetic  21.3 us (4%)
  between operations  14.3 us (3%)
  local copies, waits for them, and re-layouts  7.45 us (2%)
    all_gather x1, waiting for transfers between devices, body(): lax.all_gather(mixer_down_weight, 'sp', axis=1, tiled=True)  86.9 us
    all_gather x1, waiting for transfers between devices, body(): lax.all_gather(mixer_up_weight, 'sp', axis=0, tiled=True)  78.4 us
    all_gather x1, waiting for transfers between devices, body(): lax.all_gather(mixer_gate_weight, 'sp', axis=0, tiled=True)  70.8 us
    all_gather x2, blocking collectives, carried_in(): pieces = jax.tree.map(lambda part: lax.all_gather(part, axis), value)  41.3 us
    reduce_scatter x1, waiting for transfers between devices, body(): lax.psum_scatter(down_terms.astype(jnp.bfloat16), 'tp', scatter_dimension...  36.1 us
    reduce_scatter x1, waiting for transfers between devices, body(): lax.psum_scatter(lax.dot_general(columns, gated, (((0,), (1,)), ((), ()))...  32.8 us
    all_gather x1, waiting for transfers between devices, body(): normed_rows = lax.all_gather(normed_own, 'tp', axis=1, tiled=True)  28.1 us
    unnamed x1, blocking collectives  17.6 us
  transfers between devices with their start and end apart: 7, of which 6 were waited for; matrix products, arithmetic and copies ran while one was open for 4% of the time, Pallas kernels for 0%

commit v1 on v0

--- a/solution.py
+++ b/solution.py
@@ -185,7 +185,7 @@
     activated = (jax.nn.silu(gate_value) * up_value).astype(jnp.bfloat16)
     down_terms = jnp.dot(
         activated,
-        lax.all_gather(mixer_down_weight, "sp", axis=1, tiled=True),
+        jnp.concatenate(lax.all_gather(mixer_down_weight, "sp"), axis=1),
         preferred_element_type=jnp.float32,
     )
     channel_out = lax.psum_scatter(

time: 491 us -> 490 us (level)
  waiting for transfers between devices: 335 us -> 326 us
  local copies, waits for them, and re-layouts: 7.45 us -> 15.3 us
    all_gather x1, waiting for transfers between devices: 86.9 us -> 71.3 us  [body(): lax.all_gather(mixer_down_weight, 'sp')]
    reshape x1 -> x2, local copies, waits for them, and re-layouts: 0.01 us -> 7.88 us  [the longest x1 7.87 us: body(): jnp.concatenate(lax.all_gather(mixer_down_weight, 'sp'), axis=1)]
    all_gather x1, waiting for transfers between devices: 70.8 us -> 78.3 us  [body(): lax.all_gather(mixer_gate_weight, 'sp', axis=0, tiled=True)]
  transfers between devices with their start and end apart: 7 -> 7, of which waited for: 6 -> 6; matrix products, arithmetic and copies ran while one was open for 4% -> 5% of each run, Pallas kernels for 0% -> 0%
where the time goes in v1:
time: 490 us; the launch traced here: 489 us
  waiting for transfers between devices  326 us (67%)
  blocking collectives  70.3 us (14%)
  matrix products  41.1 us (8%)
  other arithmetic  21.3 us (4%)
  local copies, waits for them, and re-layouts  15.3 us (3%)
  between operations  14.3 us (3%)
    all_gather x1, waiting for transfers between devices, body(): lax.all_gather(mixer_up_weight, 'sp', axis=0, tiled=True)  78.3 us
    all_gather x1, waiting for transfers between devices, body(): lax.all_gather(mixer_gate_weight, 'sp', axis=0, tiled=True)  78.3 us
    all_gather x1, waiting for transfers between devices, body(): lax.all_gather(mixer_down_weight, 'sp')  71.3 us
    all_gather x2, blocking collectives, carried_in(): pieces = jax.tree.map(lambda part: lax.all_gather(part, axis), value)  41.3 us
    reduce_scatter x1, waiting for transfers between devices, body(): lax.psum_scatter(down_terms.astype(jnp.bfloat16), 'tp', scatter_dimension...  36.1 us
    reduce_scatter x1, waiting for transfers between devices, body(): lax.psum_scatter(lax.dot_general(columns, gated, (((0,), (1,)), ((), ()))...  32.3 us
    all_gather x1, waiting for transfers between devices, body(): normed_rows = lax.all_gather(normed_own, 'tp', axis=1, tiled=True)  28.1 us
    unnamed x1, blocking collectives  17.6 us
  transfers between devices with their start and end apart: 7, of which 6 were waited for; matrix products, arithmetic and copies ran while one was open for 5% of the time, Pallas kernels for 0%

profile of v1, /device:TPU:0, one launch (start us, length us, event | category | flops | bytes accessed | tf_op | source)
XLA Modules:
  0.0 489.0 jit_solution(18070727529678460058)
XLA Ops:
  9.9 1.4 copy.56
  11.4 2.8 fusion.32
  15.8 22.4 %all-gather.4 = f32[8,1,2]{2,1,0:T(1,128)S(1)} all-gather(f32[1,1,2]{2,1,0:T(1,128)S(1)} %fusion.59), channel_id=1, replica_groups=mesh['sp'=8,'tp'=4] {'sp'}, dimensions={0}, use_global_device_ids=true | all-gather | bytes 72 | tf_op jit(solution)/shard_map/all_gather | solution.py:15
  38.1 17.6 %all-reduce = f32[16]{0:T(128)S(1)} all-reduce(f32[16]{0:T(128)S(1)} %dynamic-update-slice), channel_id=2, replica_groups=mesh['sp'=8,'tp'=4] {'sp'}, use_global_device_ids=true, to_apply=%add | all-reduce | flops 16 | bytes 128
  56.2 18.9 %all-gather.5 = f32[8,2,128]{2,1,0:T(2,128)S(1)} all-gather(f32[1,2,128]{2,1,0:T(2,128)S(1)} %add_bitcast_fusion.1), channel_id=4, replica_groups=mesh['sp'=8,'tp'=4] {'sp'}, dimensions={0}, use_global_device_ids=true | all-gather | bytes 9216 | tf_op jit(solution)/shard_map/all_gather | solution.py:15
  76.4 8.3 %while.20 = (s32[]{:T(128)}, f32[2]{0:T(128)S(1)}, f32[2,256,128]{2,1,0:T(8,128)S(1)}, f32[2,128]{1,0:T(2,128)S(1)}, f32[2]{0:T(128)S(1)}, /*index=5*/s32[]{:T(1...) while((s32[]{:T(128)}, f32[2]{0:T(128)S(1)}, ...), condition=%wide.region_4.5_spmd.clone, body=%wide.region_3.4_spmd.clone.sunk | while | flops 328984 | bytes 789781 | solution.py:24
  76.4 1.1 fusion.90
  77.6 1.1 fusion.90
  78.8 1.1 fusion.90
  80.0 1.1 fusion.90
  81.2 1.1 fusion.90
  84.8 3.0 fusion.10
  88.5 1.5 fusion.37
  90.1 2.4 fusion.69
  92.9 1.5 fusion.28
  94.4 3.1 copy.48
  97.5 4.9 fusion.9
  105.3 32.3 %reduce-scatter.3.cloned.1.call-done = bf16[512,768]{0,1:T(8,128)(2,1)} async-done(((bf16[2048,768]{0,1:T(8,128)(2,1)}), bf16[512,768]{0,1:T(8,128)(2,1)}) %reduce-scatter.3.cloned.1.call-update) | async-done | bytes 786448 | tf_op jit(solution)/shard_map/reduce_scatter | solution.py:148
  137.6 1.4 fusion.15
  138.9 5.8 %psum.14 = f32[768]{0:T(1024)S(1)} all-reduce(f32[768]{0:T(1024)S(1)} %fusion.15), channel_id=1, replica_groups=mesh['sp'=8,'tp'=4] {'tp'}, use_global_device_ids=true, to_apply=%region_11.12 | all-reduce | flops 768 | bytes 6144 | tf_op jit(solution)/shard_map/psum | solution.py:159
  144.7 1.7 fusion.19
  146.7 5.7 %psum.15 = f32[768]{0:T(1024)S(1)} all-reduce(f32[768]{0:T(1024)S(1)} %fusion.20), channel_id=1, replica_groups=mesh['sp'=8,'tp'=4] {'tp'}, use_global_device_ids=true, to_apply=%region_13.14 | all-reduce | flops 768 | bytes 6144 | tf_op jit(solution)/shard_map/psum | solution.py:168
  152.3 1.1 fusion.22
  154.3 71.3 %all-gather.20.cloned.1.call-done = bf16[10240,256]{1,0:T(8,128)(2,1)} async-done(((bf16[1280,256]{1,0:T(8,128)(2,1)}), bf16[10240,256]{1,0:T(8,128)(2,1)}) %all-gather.20.cloned.1.call-update) | async-done | bytes 5242896 | tf_op jit(solution)/shard_map/all_gather | solution.py:188
  225.7 7.9 %copy.49 = bf16[1280,8,256]{0,2,1:T(8,128)(2,1)} copy(bf16[1280,8,256]{2,0,1:T(8,128)(2,1)} %bitcast.182) | data formatting | bytes 10485760 | tf_op jit(solution)/shard_map/reshape | solution.py:188
  233.6 78.3 %all-gather.14.cloned.1.call-done = bf16[2048,1280]{1,0:T(8,128)(2,1)} async-done(((bf16[256,1280]{1,0:T(8,128)(2,1)}), bf16[2048,1280]{1,0:T(8,128)(2,1)}) %all-gather.14.cloned.1.call-update) | async-done | bytes 5242896 | tf_op jit(solution)/shard_map/all_gather | solution.py:177
  311.8 28.1 %all-gather.12.cloned.1.call-done = bf16[768,2048]{1,0:T(8,128)(2,1)} async-done(((bf16[768,512]{1,0:T(8,128)(2,1)}), bf16[768,2048]{1,0:T(8,128)(2,1)}) %all-gather.12.cloned.1.call-update) | async-done | bytes 3145744 | tf_op jit(solution)/shard_map/all_gather | solution.py:173
  340.0 9.6 %fusion.72 = f32[768,1280]{1,0:T(8,128)} fusion(bf16[768,2048]{1,0:T(8,128)(2,1)} %all-gather.12.cloned.1.call-done, bf16[2048,1280]{1,0:T(8,128)(2,1)} %all-gather.14.cloned.1.call-done), kind=kOutput, calls=%fused_computation.118 | convolution fusion | flops 4026531840 | bytes 12320768 | tf_op jit(solution)/shard_map/dot_general | solution.py:175
  349.6 78.3 %all-gather.16.cloned.1.call-done = bf16[2048,1280]{1,0:T(8,128)(2,1)} async-done(((bf16[256,1280]{1,0:T(8,128)(2,1)}), bf16[2048,1280]{1,0:T(8,128)(2,1)}) %all-gather.16.cloned.1.call-update) | async-done | bytes 5242896 | tf_op jit(solution)/shard_map/all_gather | solution.py:182
  427.9 16.0 %convolution_convert_fusion.1 = bf16[768,2048]{1,0:T(8,128)(2,1)} fusion(bf16[1280,2048]{0,1:T(8,128)(2,1)} %bitcast.183, bf16[768,2048]{1,0:T(8,128)(2,1)} %all-gather.12.cloned.1.call-done, bf16[2048,1280]{1,0:T(8,128)(2,1)} %all-gather.16.cloned.1.call-done, f32[768,1280]{1,0:T(8,128)} %fusion.72), kind=kOutput, calls=%fused_computation.23 | convolution fusion | flops 8060534784 | bytes 20709376 | tf_op jit(solution)/shard_map/dot_general | solution.py:186
  443.9 36.1 %reduce-scatter.5.cloned.1.call-done = bf16[768,512]{1,0:T(8,128)(2,1)} async-done(((bf16[768,2048]{1,0:T(8,128)(2,1)}), bf16[768,512]{1,0:T(8,128)(2,1)}) %reduce-scatter.5.cloned.1.call-update) | async-done | bytes 786448 | tf_op jit(solution)/shard_map/reduce_scatter | solution.py:191
  480.0 2.2 fusion.23
  (97 shorter events, 14.2 us)
Async XLA Ops:
  6.5 91.0 %copy-start = (bf16[512,2048]{1,0:T(8,128)(2,1)S(1)}, bf16[512,2048]{1,0:T(8,128)(2,1)}, u32[]{:S(2)}) copy-start(bf16[512,2048]{1,0:T(8,128)(2,1)} %param.26) | copy-start | bytes 6291460
  6.5 7.8 %copy-start.8 = (u32[32]{0:T(128)S(1)}, u32[32]{0:T(128)}, u32[]{:S(2)}) copy-start(u32[32]{0:T(128)} %constant.77) | copy-start | bytes 388
  6.5 49.4 %copy-start.4 = (bf16[768,256]{1,0:T(8,128)(2,1)S(1)}, bf16[768,256]{1,0:T(8,128)(2,1)}, u32[]{:S(2)}) copy-start(bf16[768,256]{1,0:T(8,128)(2,1)} %param.19) | copy-start | bytes 1179652
  6.5 49.3 %copy-start.6 = (f32[512]{0:T(512)S(1)}, f32[512]{0:T(512)}, u32[]{:S(2)}) copy-start(f32[512]{0:T(512)} %param.25) | copy-start | bytes 6148
  6.5 69.8 %all-gather.18.cloned.1.call-start = ((), (), s32[]{:S(2)}) async-start(), calls=%async_computation.7 | async-start | bytes 2359296 | tf_op jit(solution)/shard_map/all_gather | solution.py:15
  7.5 67.9 %copy-start.5 = (f32[768,2]{0,1:T(2,128)S(1)}, f32[768,2]{0,1:T(2,128)}, u32[]{:S(2)}) copy-start(f32[768,2]{0,1:T(2,128)} %param.22) | copy-start | bytes 18436
  11.3 26.8 %copy-start.1 = (bf16[768,512]{0,1:T(8,128)(2,1)}, bf16[768,512]{0,1:T(8,128)(2,1)S(1)}, u32[]{:S(2)}) copy-start(bf16[768,512]{0,1:T(8,128)(2,1)S(1)} %copy.56) | copy-start | bytes 2359300
  14.3 123.3 %reduce-scatter.3.cloned.1.call-start = ((), (), s32[]{:S(2)}) async-start(), calls=%async_computation.2 | async-start | bytes 3932160 | tf_op jit(solution)/shard_map/reduce_scatter | solution.py:148
  75.4 9.4 %copy-start.3 = (bf16[768,256]{1,0:T(8,128)(2,1)S(1)}, bf16[768,256]{1,0:T(8,128)(2,1)}, u32[]{:S(2)}) copy-start(bf16[768,256]{1,0:T(8,128)(2,1)} %param.18) | copy-start | bytes 1179652
  87.7 2.4 copy-start.2
  94.4 3.1 copy-start.7
  102.4 123.3 %all-gather.20.cloned.1.call-start = ((), (), s32[]{:S(2)}) async-start(), calls=%async_computation.8 | async-start | bytes 5898240 | tf_op jit(solution)/shard_map/all_gather | solution.py:188
  103.2 208.7 %all-gather.14.cloned.1.call-start = ((), (), s32[]{:S(2)}) async-start(), calls=%async_computation.4 | async-start | bytes 5898240 | tf_op jit(solution)/shard_map/all_gather | solution.py:177
  103.7 236.2 %all-gather.12.cloned.1.call-start = ((), (), s32[]{:S(2)}) async-start(), calls=%async_computation.3 | async-start | bytes 3932160 | tf_op jit(solution)/shard_map/all_gather | solution.py:173
  153.5 274.4 %all-gather.16.cloned.1.call-start = ((), (), s32[]{:S(2)}) async-start(), calls=%async_computation.5 | async-start | bytes 5898240 | tf_op jit(solution)/shard_map/all_gather | solution.py:182
  154.1 325.9 %reduce-scatter.5.cloned.1.call-start = ((), (), s32[]{:S(2)}) async-start(), calls=%async_computation.6 | async-start | bytes 3932160 | tf_op jit(solution)/shard_map/reduce_scatter | solution.py:191
Sparse Core Ops, SparseCore 0:
  14.4 52.0 all-gather.17
  102.5 34.9 reduce-scatter.2
  139.8 85.8 all-gather.19
  227.7 84.0 all-gather.13
  313.2 26.6 all-gather.11
  342.0 85.8 all-gather.15
  444.0 35.8 reduce-scatter.4
